TPU v7x, 32 devices: a whole 2x2x4 slice. The times are simulated.
32 devices in a mesh: ep: 4 (over z), tp: 8 (over y, x, core).
Axes of the slice: x: 2, y: 2, z: 4, core: 2. Of those that a mesh axis runs over, the one named last changes fastest.
Arguments:
- hidden_in: bfloat16 [48, 2048], P('ep', 'tp'), may hold values from -12 to 12
- state: float32 [48, 32, 128, 128], P('ep', 'tp'), may hold values from -3 to 3
- lower_bound: float32 [32, 128], P('tp'), may hold values from 0.05 to 0.95
- w_forget: bfloat16 [2048, 4096], P(None, 'tp'), may hold values from -0.125 to 0.125
- w_input: bfloat16 [2048, 4096], P(None, 'tp'), may hold values from -0.125 to 0.125
- w_query: bfloat16 [2048, 4096], P(None, 'tp'), may hold values from -0.125 to 0.125
- w_outgate: bfloat16 [2048, 4096], P(None, 'tp'), may hold values from -0.125 to 0.125
- head_gain: float32 [128], replicated, may hold values from 0.1 to 1.9
- w_out: bfloat16 [4096, 2048], P('tp'), may hold values from -0.125 to 0.125
- ln1_gain: float32 [2048], replicated, may hold values from 0.1 to 8
- ln1_bias: float32 [2048], replicated, may hold values from -1.5 to 1.5
- routes: int32 [48, 4], P('ep'), may hold values from 0 to 7, all different within a row; in each aligned block of 12 rows (0 to 11, 12 to 23, ...) at most 9 rows name the same one
- route_weights: float32 [48, 4], P('ep'), may hold values from 0.2 to 1.5
- exp_gate: bfloat16 [8, 2048, 4096], P('ep', None, 'tp'), may hold values from -0.125 to 0.125
- exp_up: bfloat16 [8, 2048, 4096], P('ep', None, 'tp'), may hold values from -0.125 to 0.125
- exp_down: bfloat16 [8, 4096, 2048], P('ep', 'tp'), may hold values from -0.125 to 0.125
- sh_gate: bfloat16 [2048, 512], P(None, 'tp'), may hold values from -0.125 to 0.125
- sh_up: bfloat16 [2048, 512], P(None, 'tp'), may hold values from -0.125 to 0.125
- sh_down: bfloat16 [512, 2048], P('tp'), may hold values from -0.25 to 0.25
- ln2_gain: float32 [2048], replicated, may hold values from 0.1 to 1.9
- ln2_bias: float32 [2048], replicated, may hold values from -1.5 to 1.5
Outputs:
- mixed_out: bfloat16 [48, 2048], P('ep', 'tp')
- new_state: float32 [48, 32, 128, 128], P('ep', 'tp')
Inputs may be any that keep to these rules, and one draw needn't show every extreme that they name: `routes`: each row names 4 different experts; among the rows of one index of ep (12 rows) no expert is named more than 9 times, a bound that some block reaches.
All inputs are finite; a program needn't handle non-finite values.
Results may differ from a plain program's by a relative error of at most 0.023.
Values may be sent and summed in bfloat16 or wider, within the bound.
A program may use at most 64 MiB of HBM per device.

v0:
```python
import jax
import jax.numpy as jnp
from jax import lax
from jax.sharding import PartitionSpec as P

EPS = 1e-05
ALPHA = 2.0**0.25


def rounded(value):
    return lax.optimization_barrier(value.astype(jnp.bfloat16)).astype(jnp.float32)


def local(
    hidden_in,
    state,
    lower_bound,
    w_forget,
    w_input,
    w_query,
    w_outgate,
    head_gain,
    w_out,
    ln1_gain,
    ln1_bias,
    routes,
    route_weights,
    exp_gate,
    exp_up,
    exp_down,
    sh_gate,
    sh_up,
    sh_down,
    ln2_gain,
    ln2_bias,
):
    n_tp = lax.axis_size("tp")
    n_ep = lax.axis_size("ep")
    seq_count = hidden_in.shape[0]
    col_count = hidden_in.shape[1]
    model_width = col_count * n_tp
    col_start = lax.axis_index("tp") * col_count
    heads_dev = state.shape[1]
    head_size = state.shape[2]
    top_count = routes.shape[1]
    local_experts = exp_gate.shape[0]
    expert_count = local_experts * n_ep
    capacity = max(2, 3 * seq_count * top_count // (2 * expert_count))
    slot_count = expert_count * capacity
    rows_full = lax.all_gather(hidden_in, "tp", axis=1, tiled=True)

    def project(weight):
        product = jnp.dot(rows_full, weight, preferred_element_type=jnp.float32)
        return rounded(product).reshape(seq_count, heads_dev, head_size)

    forget_pre = project(w_forget)
    forget = lower_bound + (1.0 - lower_bound) * jax.nn.sigmoid(forget_pre)
    key_part = (1.0 - lower_bound) * jax.nn.sigmoid(-forget_pre)
    values = project(w_input)
    queries = jax.nn.silu(project(w_query))
    out_gate = jax.nn.silu(project(w_outgate))
    new_state = forget[..., None] * state + key_part[..., None] * values[:, :, None, :]
    readout = jnp.einsum("bhd,bhdv->bhv", queries, new_state, precision=lax.Precision.HIGHEST)
    normed = readout * lax.rsqrt(jnp.mean(readout * readout, -1, keepdims=True) + EPS) * head_gain
    mixed = (normed * out_gate).astype(jnp.bfloat16).reshape(seq_count, heads_dev * head_size)
    branch = jnp.dot(mixed, w_out, preferred_element_type=jnp.float32)
    summed = lax.psum(branch.astype(jnp.bfloat16), "tp").astype(jnp.float32)
    residual = ALPHA * rows_full.astype(jnp.float32) + summed
    average = jnp.mean(residual, -1, keepdims=True)
    centered = residual - average
    variance = jnp.mean(centered * centered, -1, keepdims=True)
    normed_rows = (centered * lax.rsqrt(variance + EPS) * ln1_gain + ln1_bias).astype(jnp.bfloat16)
    routes_flat = routes.reshape(-1)
    one_hot = (routes_flat[:, None] == jnp.arange(expert_count, dtype=jnp.int32)[None, :]).astype(
        jnp.int32
    )
    position = jnp.sum((jnp.cumsum(one_hot, 0) - one_hot) * one_hot, 1)
    slot_index = routes_flat * capacity + position
    placing = (slot_index[:, None] == jnp.arange(slot_count, dtype=jnp.int32)[None, :]).astype(
        jnp.float32
    )
    chooser = jnp.sum(placing.reshape(seq_count, top_count, slot_count), 1).astype(jnp.bfloat16)
    weighted = jnp.sum(
        (placing * route_weights.reshape(-1)[:, None]).reshape(seq_count, top_count, slot_count), 1
    )
    own_cols = lax.dynamic_slice_in_dim(normed_rows, col_start, col_count, 1)
    picked = lax.dot_general(
        chooser, normed_rows, (((0,), (0,)), ((), ())), preferred_element_type=jnp.float32
    )
    arrived = lax.all_to_all(
        picked.astype(jnp.bfloat16).reshape(n_ep, local_experts * capacity, normed_rows.shape[1]),
        "ep",
        split_axis=0,
        concat_axis=0,
        tiled=True,
    )
    blocks = arrived.reshape(n_ep, local_experts, capacity, model_width)
    gate_part = jnp.einsum("gecd,edf->gecf", blocks, exp_gate, preferred_element_type=jnp.float32)
    up_part = jnp.einsum("gecd,edf->gecf", blocks, exp_up, preferred_element_type=jnp.float32)
    hidden_part = (jax.nn.silu(gate_part) * up_part).astype(jnp.bfloat16)
    expert_part = jnp.einsum(
        "gecf,efd->gecd", hidden_part, exp_down, preferred_element_type=jnp.float32
    )
    expert_part = expert_part.reshape(n_ep, local_experts * capacity, model_width).astype(
        jnp.bfloat16
    )
    shared_hidden = (
        jax.nn.silu(jnp.dot(normed_rows, sh_gate, preferred_element_type=jnp.float32))
        * jnp.dot(normed_rows, sh_up, preferred_element_type=jnp.float32)
    ).astype(jnp.bfloat16)
    shared_part = jnp.dot(shared_hidden, sh_down, preferred_element_type=jnp.float32)
    returned = lax.all_to_all(expert_part, "ep", split_axis=0, concat_axis=0, tiled=True)
    routed_partial = jnp.dot(
        weighted,
        returned.reshape(slot_count, model_width).astype(jnp.float32),
        precision=lax.Precision.HIGHEST,
    )
    combined = lax.psum_scatter(
        (routed_partial + shared_part).astype(jnp.bfloat16), "tp", scatter_dimension=1, tiled=True
    ).astype(jnp.float32)
    final_in = ALPHA * own_cols.astype(jnp.float32) + combined
    moments_two = lax.psum((jnp.sum(final_in, -1), jnp.sum(final_in * final_in, -1)), "tp")
    average_two = moments_two[0][:, None] / model_width
    variance_two = moments_two[1][:, None] / model_width - average_two * average_two
    gain_two = lax.dynamic_slice_in_dim(ln2_gain, col_start, col_count)
    bias_two = lax.dynamic_slice_in_dim(ln2_bias, col_start, col_count)
    mixed_out = (
        (final_in - average_two) * lax.rsqrt(variance_two + EPS) * gain_two + bias_two
    ).astype(jnp.bfloat16)
    return (mixed_out, new_state)


def solution(mesh):
    placed = (
        P("ep", "tp"),
        P("ep", "tp", None, None),
        P("tp", None),
        P(None, "tp"),
        P(None, "tp"),
        P(None, "tp"),
        P(None, "tp"),
        P(),
        P("tp", None),
        P(),
        P(),
        P("ep", None),
        P("ep", None),
        P("ep", None, "tp"),
        P("ep", None, "tp"),
        P("ep", "tp", None),
        P(None, "tp"),
        P(None, "tp"),
        P("tp", None),
        P(),
        P(),
    )
    return jax.shard_map(
        local,
        mesh=mesh,
        in_specs=placed,
        out_specs=(P("ep", "tp"), P("ep", "tp", None, None)),
        check_vma=False,
    )
```

profile of v0, /device:TPU:0, one launch (start us, length us, event | category | flops | bytes accessed | tf_op | source)
XLA Modules:
  0.0 155.0 jit_solution(1456552702936218920)
XLA Ops:
  7.2 0.9 copy.41
  8.6 0.8 copy.43
  9.4 10.7 %all_gather.3 = bf16[12,2048]{1,0:T(8,128)(2,1)S(1)} all-gather(bf16[12,256]{1,0:T(8,128)(2,1)} %param.21), channel_id=1, replica_groups=mesh['ep'=4,'tp'=8] {'tp'}, dimensions={1}, use_global_device_ids=true | all-gather | bytes 55296 | tf_op jit(solution)/shard_map/all_gather | solution.py:50
  20.1 2.0 %convolution_convert_fusion.2 = bf16[12,512]{1,0:T(8,128)(2,1)S(1)} fusion(bf16[12,2048]{1,0:T(8,128)(2,1)S(1)} %all_gather.3, bf16[2048,512]{1,0:T(8,128)(2,1)} %param.27), kind=kOutput, calls=%fused_computation.17 | convolution fusion | flops 25171968 | bytes 2158592 | tf_op jit(solution)/shard_map/dot_general | solution.py:53
  22.1 2.0 %convolution_convert_fusion.5 = bf16[12,512]{1,0:T(8,128)(2,1)S(1)} fusion(bf16[12,2048]{1,0:T(8,128)(2,1)S(1)} %all_gather.3, bf16[2048,512]{1,0:T(8,128)(2,1)} %param.26), kind=kOutput, calls=%fused_computation.20 | convolution fusion | flops 25171968 | bytes 2158592 | tf_op jit(solution)/shard_map/dot_general | solution.py:53
  24.1 2.0 %convolution_convert_fusion.3 = bf16[12,512]{1,0:T(8,128)(2,1)S(1)} fusion(bf16[12,2048]{1,0:T(8,128)(2,1)S(1)} %all_gather.3, bf16[2048,512]{1,0:T(8,128)(2,1)} %param.25), kind=kOutput, calls=%fused_computation.18 | convolution fusion | flops 25171968 | bytes 2158592 | tf_op jit(solution)/shard_map/dot_general | solution.py:53
  26.1 2.0 %convolution_convert_fusion.4 = bf16[12,512]{1,0:T(8,128)(2,1)S(1)} fusion(bf16[12,2048]{1,0:T(8,128)(2,1)S(1)} %all_gather.3, bf16[2048,512]{1,0:T(8,128)(2,1)} %param.24), kind=kOutput, calls=%fused_computation.19 | convolution fusion | flops 25171968 | bytes 2158592 | tf_op jit(solution)/shard_map/dot_general | solution.py:53
  28.3 3.8 %multiply_add_fusion = f32[12,4,128,128]{3,2,1,0:T(8,128)S(1)} fusion(f32[12,4,128,128]{3,2,1,0:T(8,128)} %param.22, f32[12,4,128]{2,1,0:T(4,128)S(1)} %reshape.140, f32[12,4,128]{2,1,0:T(4,128)S(1)} %bitcast.85, f32[12,4,128]{2,1,0:T(4,128)S(1)} %bitcast.84), kind=kLoop, calls=%fused_computation.6 | loop fusion | flops 2359296 | bytes 6365184 | tf_op jit(solution)/shard_map/add | solution.py:62
  32.1 1.6 %copy-done.1 = f32[12,4,128,128]{3,2,1,0:T(8,128)} copy-done((f32[12,4,128,128]{3,2,1,0:T(8,128)}, f32[12,4,128,128]{3,2,1,0:T(8,128)S(1)}, u32[]{:S(2)}) %copy-start.1) | copy-done | bytes 3145752
  33.7 2.8 %fusion.51 = f32[12,4,1,128]{3,2,1,0:T(1,128)S(1)} fusion(f32[12,4,128,1]{2,3,1,0:T(1,128)S(1)} %bitcast.83, f32[12,4,128,128]{3,2,1,0:T(8,128)S(1)} %multiply_add_fusion), kind=kOutput, calls=%fused_computation.69 | convolution fusion | flops 9437184 | bytes 3194880 | tf_op jit(solution)/shard_map/bhd,bhdv->bhv/dot_general | solution.py:63
  37.1 23.9 %psum.21 = bf16[12,2048]{1,0:T(8,128)(2,1)S(1)} all-reduce(bf16[12,2048]{1,0:T(8,128)(2,1)S(1)} %convolution_convert_fusion.1), channel_id=1, replica_groups=mesh['ep'=4,'tp'=8] {'tp'}, use_global_device_ids=true, to_apply=%region_1.2 | all-reduce | flops 24576 | bytes 98304 | tf_op jit(solution)/shard_map/psum | solution.py:67
  62.0 13.9 %all_to_all.10 = bf16[4,18,2048]{2,1,0:T(8,128)(2,1)S(1)} all-to-all(bf16[4,18,2048]{2,1,0:T(8,128)(2,1)S(1)} %reshape.135), channel_id=1, replica_groups=mesh['ep'=4,'tp'=8] {'ep'}, dimensions={0} | all-to-all | bytes 589824 | tf_op jit(solution)/shard_map/all_to_all | solution.py:90
  76.0 2.9 %fusion.13 = f32[4,2,9,512]{3,2,0,1:T(8,128)S(1)} fusion(bf16[2,2048,512]{2,1,0:T(8,128)(2,1)} %param.34, bf16[4,2,9,2048]{3,0,2,1:T(4,128)(2,1)S(1)} %bitcast.78), kind=kOutput, calls=%fused_computation.13 | convolution fusion | flops 150994944 | bytes 4636672 | tf_op jit(solution)/shard_map/gecd,edf->gecf/dot_general | solution.py:98
  79.0 5.0 %fusion.9 = bf16[4,2,9,2048]{3,2,0,1:T(8,128)(2,1)S(1)} fusion(bf16[2,512,2048]{2,1,0:T(8,128)(2,1)} %param.36, bf16[2,2048,512]{2,1,0:T(8,128)(2,1)} %param.35, bf16[4,2,9,2048]{3,0,2,1:T(4,128)(2,1)S(1)} %bitcast.79, f32[4,2,9,512]{3,2,0,1:T(8,128)S(1)} %fusion.13), kind=kOutput, calls=%fused_computation.8 | convolution fusion | flops 302358528 | bytes 9125888 | tf_op jit(solution)/shard_map/gecf,efd->gecd/dot_general | solution.py:101
  84.2 0.9 copy.48
  85.2 3.5 %all-to-all-start.1 = ((bf16[4,18,2048]{2,1,0:T(8,128)(2,1)}), bf16[4,18,2048]{2,1,0:T(8,128)(2,1)S(1)}, u32[]{:S(2)}, u32[]{:S(2)}) async-start(bf16[4,18,2048]{2,1,0:T(8,128)(2,1)} %copy.48), calls=%async_computation.1 | async-start | bytes 786432 | tf_op jit(solution)/shard_map/all_to_all | solution.py:112
  88.7 1.1 fusion.53
  89.8 8.4 %all-to-all-done.1 = bf16[4,18,2048]{2,1,0:T(8,128)(2,1)S(1)} async-done(((bf16[4,18,2048]{2,1,0:T(8,128)(2,1)}), bf16[4,18,2048]{2,1,0:T(8,128)(2,1)S(1)}, u32[]{:S(2)}, u32[]{:S(2)}) %all-to-all-start.1) | async-done | bytes 294944 | tf_op jit(solution)/shard_map/all_to_all | solution.py:112
  98.5 2.0 %fusion.12 = bf16[12,2048]{1,0:T(8,128)(2,1)} fusion(f32[12,2048]{1,0:T(8,128)S(1)} %fusion.52, bf16[64,2048]{1,0:T(8,128)(2,1)S(1)} %copy-done.2, bf16[12,2048]{1,0:T(8,128)(2,1)S(1)} %add_convert_fusion, bf16[2048,64]{0,1:T(8,128)(2,1)} %param.38, f32[12,64]{1,0:T(8,128)S(1)} %fusion.53), kind=kOutput, calls=%fused_computation.11 | convolution fusion | flops 6345216 | bytes 723968 | tf_op jit(solution)/shard_map/dot_general | solution.py:111
  100.5 0.8 dynamic_slice.11
  102.0 31.7 %reduce-scatter.2.cloned.1.call-done = bf16[12,256]{1,0:T(8,128)(2,1)} async-done(((bf16[12,2048]{1,0:T(8,128)(2,1)}), bf16[12,256]{1,0:T(8,128)(2,1)}) %reduce-scatter.2.cloned.1.call-update) | async-done | bytes 6160 | tf_op jit(solution)/shard_map/reduce_scatter | solution.py:118
  133.8 0.8 fusion.41
  134.6 12.2 %all-reduce = (f32[12]{0:T(128)S(1)}, f32[12]{0:T(128)S(1)}) all-reduce(f32[12]{0:T(128)S(1)} %get-tuple-element.3, f32[12]{0:T(128)S(1)} %get-tuple-element.2), channel_id=1, replica_groups=mesh['ep'=4,'tp'=8] {'tp'}, use_global_device_ids=true, to_apply=%region_12.13 | all-reduce | flops 24 | bytes 192 | tf_op jit(solution)/shard_map/psum | solution.py:122
  146.8 1.4 add_convert_fusion.1
  (52 shorter events, 3.9 us)
Async XLA Ops:
  7.2 29.6 %copy-start = (bf16[512,2048]{1,0:T(8,128)(2,1)S(1)}, bf16[512,2048]{1,0:T(8,128)(2,1)}, u32[]{:S(2)}) copy-start(bf16[512,2048]{1,0:T(8,128)(2,1)} %param.29) | copy-start | bytes 6291460
  22.1 6.1 %copy-start.3 = (f32[4,128]{1,0:T(4,128)S(1)}, f32[4,128]{1,0:T(4,128)}, u32[]{:S(2)}) copy-start(f32[4,128]{1,0:T(4,128)} %param.23) | copy-start | bytes 6148
  32.1 1.7 %copy-start.1 = (f32[12,4,128,128]{3,2,1,0:T(8,128)}, f32[12,4,128,128]{3,2,1,0:T(8,128)S(1)}, u32[]{:S(2)}) copy-start(f32[12,4,128,128]{3,2,1,0:T(8,128)S(1)} %multiply_add_fusion) | copy-start | bytes 9437188
  32.1 4.5 %copy-start.6 = (f32[128]{0:T(128)S(1)}, f32[128]{0:T(128)}, u32[]{:S(2)}) copy-start(f32[128]{0:T(128)} %param.28) | copy-start | bytes 1540
  32.1 29.4 %copy-start.4 = (f32[2048]{0:T(1024)S(1)}, f32[2048]{0:T(1024)}, u32[]{:S(2)}) copy-start(f32[2048]{0:T(1024)} %param.31) | copy-start | bytes 24580
  32.1 29.4 %copy-start.5 = (f32[2048]{0:T(1024)S(1)}, f32[2048]{0:T(1024)}, u32[]{:S(2)}) copy-start(f32[2048]{0:T(1024)} %param.30) | copy-start | bytes 24580
  84.0 14.5 %copy-start.2 = (bf16[64,2048]{1,0:T(8,128)(2,1)S(1)}, bf16[64,2048]{1,0:T(8,128)(2,1)}, u32[]{:S(2)}) copy-start(bf16[64,2048]{1,0:T(8,128)(2,1)} %param.39) | copy-start | bytes 786436
  85.2 13.0 %all-to-all-start.1 = ((bf16[4,18,2048]{2,1,0:T(8,128)(2,1)}), bf16[4,18,2048]{2,1,0:T(8,128)(2,1)S(1)}, u32[]{:S(2)}, u32[]{:S(2)}) async-start(bf16[4,18,2048]{2,1,0:T(8,128)(2,1)} %copy.48), calls=%async_computation.1 | async-start | bytes 786432 | tf_op jit(solution)/shard_map/all_to_all | solution.py:112
  88.6 45.2 %reduce-scatter.2.cloned.1.call-start = ((), (), s32[]{:S(2)}) async-start(), calls=%async_computation.3 | async-start | bytes 73728 | tf_op jit(solution)/shard_map/reduce_scatter | solution.py:118
Sparse Core Ops, SparseCore 0:
  100.6 33.1 reduce-scatter.1
where the time goes:
time: 156 us; the launch traced here: 155 us
  blocking collectives  60.6 us (39%)
  waiting for transfers between devices  40.1 us (26%)
  matrix products  22.5 us (14%)
  between operations  14.3 us (9%)
  other arithmetic  7.16 us (5%)
  local copies, waits for them, and re-layouts  6.75 us (4%)
  starting transfers between devices  3.5 us (2%)
    reduce_scatter x1, waiting for transfers between devices, local(): lax.psum_scatter((routed_partial + shared_part).astype(jnp.bfloat16), 'tp...  31.7 us
    psum x1, blocking collectives, local(): summed = lax.psum(branch.astype(jnp.bfloat16), 'tp').astype(jnp.float32)  23.9 us
    all_to_all x1, blocking collectives, local(): lax.all_to_all(picked.astype(jnp.bfloat16).reshape(n_ep, local_experts *...  13.9 us
    psum x1, blocking collectives, local(): lax.psum((jnp.sum(final_in, -1), jnp.sum(final_in * final_in, -1)), 'tp')  12.2 us
    all_gather x1, blocking collectives, local(): rows_full = lax.all_gather(hidden_in, 'tp', axis=1, tiled=True)  10.7 us
    all_to_all x1, waiting for transfers between devices, local(): lax.all_to_all(expert_part, 'ep', split_axis=0, concat_axis=0, tiled=True)  8.36 us
    dot_general x4, matrix products, project(): product = jnp.dot(rows_full, weight, preferred_element_type=jnp.float32)  7.85 us
    dot_general x1, matrix products, local(): jnp.einsum('gecf,efd->gecd', hidden_part, exp_down, preferred_element_typ...  4.99 us
  transfers between devices with their start and end apart: 2, of which 2 were waited for; matrix products, arithmetic and copies ran while one was open for 2% of the time, Pallas kernels for 0%

commit v1 on v0

--- a/solution.py
+++ b/solution.py
@@ -1,10 +1,19 @@
+import functools
 import jax
 import jax.numpy as jnp
 from jax import lax
 from jax.sharding import PartitionSpec as P
+from jax.lax import all_gather
 
 EPS = 1e-05
 ALPHA = 2.0**0.25
+
+
+def search_axis_part(local_array, shard_axis):
+    return all_gather(local_array, axis_name=shard_axis).sum(axis=0)
+
+
+direct_knots_on_mesh = functools.partial(search_axis_part, shard_axis="tp")
 
 
 def rounded(value):
@@ -64,7 +73,7 @@
     normed = readout * lax.rsqrt(jnp.mean(readout * readout, -1, keepdims=True) + EPS) * head_gain
     mixed = (normed * out_gate).astype(jnp.bfloat16).reshape(seq_count, heads_dev * head_size)
     branch = jnp.dot(mixed, w_out, preferred_element_type=jnp.float32)
-    summed = lax.psum(branch.astype(jnp.bfloat16), "tp").astype(jnp.float32)
+    summed = direct_knots_on_mesh(branch.astype(jnp.bfloat16)).astype(jnp.float32)
     residual = ALPHA * rows_full.astype(jnp.float32) + summed
     average = jnp.mean(residual, -1, keepdims=True)
     centered = residual - average

time: 156 us -> 143 us (0.917)
  blocking collectives: 60.6 us -> 49.4 us
  waiting for transfers between devices: 40.1 us -> 38.3 us
    psum x1 -> x0, blocking collectives: 23.9 us -> none  [local(): summed = lax.psum(branch.astype(jnp.bfloat16), 'tp').astype(jnp.float32)]
    all_gather x0 -> x1, blocking collectives: none -> 9.67 us  [search_axis_part(): return all_gather(local_array, axis_name=shard_axis).sum(axis=0)]
    reduce_scatter x1, waiting for transfers between devices: 31.7 us -> 28.1 us  [local(): lax.psum_scatter((routed_partial + shared_part).astype(jnp.bfloat16), 'tp...]
    all_to_all x1, blocking collectives: 13.9 us -> 16.9 us  [local(): lax.all_to_all(picked.astype(jnp.bfloat16).reshape(n_ep, local_experts *...]
    all_to_all x1, waiting for transfers between devices: 8.36 us -> 10.1 us  [local(): lax.all_to_all(expert_part, 'ep', split_axis=0, concat_axis=0, tiled=True)]
where the time goes in v1:
time: 143 us; the launch traced here: 142 us
  blocking collectives  49.4 us (35%)
  waiting for transfers between devices  38.3 us (27%)
  matrix products  22.5 us (16%)
  between operations  14.3 us (10%)
  other arithmetic  7.25 us (5%)
  local copies, waits for them, and re-layouts  6.77 us (5%)
  starting transfers between devices  3.5 us (2%)
    reduce_scatter x1, waiting for transfers between devices, local(): lax.psum_scatter((routed_partial + shared_part).astype(jnp.bfloat16), 'tp...  28.1 us
    all_to_all x1, blocking collectives, local(): lax.all_to_all(picked.astype(jnp.bfloat16).reshape(n_ep, local_experts *...  16.9 us
    psum x1, blocking collectives, local(): lax.psum((jnp.sum(final_in, -1), jnp.sum(final_in * final_in, -1)), 'tp')  12.1 us
    all_gather x1, blocking collectives, local(): rows_full = lax.all_gather(hidden_in, 'tp', axis=1, tiled=True)  10.7 us
    all_to_all x1, waiting for transfers between devices, local(): lax.all_to_all(expert_part, 'ep', split_axis=0, concat_axis=0, tiled=True)  10.1 us
    all_gather x1, blocking collectives, search_axis_part(): return all_gather(local_array, axis_name=shard_axis).sum(axis=0)  9.67 us
    dot_general x4, matrix products, project(): product = jnp.dot(rows_full, weight, preferred_element_type=jnp.float32)  7.85 us
    dot_general x1, matrix products, local(): jnp.einsum('gecf,efd->gecd', hidden_part, exp_down, preferred_element_typ...  5 us
  transfers between devices with their start and end apart: 2, of which 2 were waited for; matrix products, arithmetic and copies ran while one was open for 2% of the time, Pallas kernels for 0%

profile of v1, /device:TPU:0, one launch (start us, length us, event | category | flops | bytes accessed | tf_op | source)
XLA Modules:
  0.0 142.0 jit_solution(15201163073139681216)
XLA Ops:
  7.2 0.9 copy.41
  8.6 0.8 copy.43
  9.4 10.7 %all_gather.9 = bf16[12,2048]{1,0:T(8,128)(2,1)S(1)} all-gather(bf16[12,256]{1,0:T(8,128)(2,1)} %param.21), channel_id=1, replica_groups=mesh['ep'=4,'tp'=8] {'tp'}, dimensions={1}, use_global_device_ids=true | all-gather | bytes 55296 | tf_op jit(solution)/shard_map/all_gather | solution.py:59
  20.1 2.0 %convolution_convert_fusion.2 = bf16[12,512]{1,0:T(8,128)(2,1)S(1)} fusion(bf16[12,2048]{1,0:T(8,128)(2,1)S(1)} %all_gather.9, bf16[2048,512]{1,0:T(8,128)(2,1)} %param.27), kind=kOutput, calls=%fused_computation.18 | convolution fusion | flops 25171968 | bytes 2158592 | tf_op jit(solution)/shard_map/dot_general | solution.py:62
  22.1 2.0 %convolution_convert_fusion.5 = bf16[12,512]{1,0:T(8,128)(2,1)S(1)} fusion(bf16[12,2048]{1,0:T(8,128)(2,1)S(1)} %all_gather.9, bf16[2048,512]{1,0:T(8,128)(2,1)} %param.26), kind=kOutput, calls=%fused_computation.21 | convolution fusion | flops 25171968 | bytes 2158592 | tf_op jit(solution)/shard_map/dot_general | solution.py:62
  24.1 2.0 %convolution_convert_fusion.3 = bf16[12,512]{1,0:T(8,128)(2,1)S(1)} fusion(bf16[12,2048]{1,0:T(8,128)(2,1)S(1)} %all_gather.9, bf16[2048,512]{1,0:T(8,128)(2,1)} %param.25), kind=kOutput, calls=%fused_computation.19 | convolution fusion | flops 25171968 | bytes 2158592 | tf_op jit(solution)/shard_map/dot_general | solution.py:62
  26.1 2.0 %convolution_convert_fusion.4 = bf16[12,512]{1,0:T(8,128)(2,1)S(1)} fusion(bf16[12,2048]{1,0:T(8,128)(2,1)S(1)} %all_gather.9, bf16[2048,512]{1,0:T(8,128)(2,1)} %param.24), kind=kOutput, calls=%fused_computation.20 | convolution fusion | flops 25171968 | bytes 2158592 | tf_op jit(solution)/shard_map/dot_general | solution.py:62
  28.3 3.8 %multiply_add_fusion = f32[12,4,128,128]{3,2,1,0:T(8,128)S(1)} fusion(f32[12,4,128,128]{3,2,1,0:T(8,128)} %param.22, f32[12,4,128]{2,1,0:T(4,128)S(1)} %reshape.140, f32[12,4,128]{2,1,0:T(4,128)S(1)} %bitcast.87, f32[12,4,128]{2,1,0:T(4,128)S(1)} %bitcast.86), kind=kLoop, calls=%fused_computation.6 | loop fusion | flops 2359296 | bytes 6365184 | tf_op jit(solution)/shard_map/add | solution.py:71
  32.1 1.6 %copy-done.1 = f32[12,4,128,128]{3,2,1,0:T(8,128)} copy-done((f32[12,4,128,128]{3,2,1,0:T(8,128)}, f32[12,4,128,128]{3,2,1,0:T(8,128)S(1)}, u32[]{:S(2)}) %copy-start.1) | copy-done | bytes 3145752
  33.7 2.8 %fusion.52 = f32[12,4,1,128]{3,2,1,0:T(1,128)S(1)} fusion(f32[12,4,128,1]{2,3,1,0:T(1,128)S(1)} %bitcast.85, f32[12,4,128,128]{3,2,1,0:T(8,128)S(1)} %multiply_add_fusion), kind=kOutput, calls=%fused_computation.70 | convolution fusion | flops 9437184 | bytes 3194880 | tf_op jit(solution)/shard_map/bhd,bhdv->bhv/dot_general | solution.py:72
  37.1 9.7 %all-gather.1 = bf16[8,12,2048]{2,1,0:T(8,128)(2,1)S(1)} all-gather(bf16[1,12,2048]{2,1,0:T(8,128)(2,1)S(1)} %fusion.13), channel_id=2, replica_groups=mesh['ep'=4,'tp'=8] {'tp'}, dimensions={0}, use_global_device_ids=true | all-gather | bytes 442368 | tf_op jit(solution)/shard_map/all_gather | solution.py:13
  47.9 16.9 %all_to_all.10 = bf16[4,18,2048]{2,1,0:T(8,128)(2,1)S(1)} all-to-all(bf16[4,18,2048]{2,1,0:T(8,128)(2,1)S(1)} %reshape.135), channel_id=1, replica_groups=mesh['ep'=4,'tp'=8] {'ep'}, dimensions={0} | all-to-all | bytes 589824 | tf_op jit(solution)/shard_map/all_to_all | solution.py:99
  65.0 2.9 %fusion.14 = f32[4,2,9,512]{3,2,0,1:T(8,128)S(1)} fusion(bf16[2,2048,512]{2,1,0:T(8,128)(2,1)} %param.34, bf16[4,2,9,2048]{3,0,2,1:T(4,128)(2,1)S(1)} %bitcast.80), kind=kOutput, calls=%fused_computation.14 | convolution fusion | flops 150994944 | bytes 4636672 | tf_op jit(solution)/shard_map/gecd,edf->gecf/dot_general | solution.py:107
  67.9 5.0 %fusion.9 = bf16[4,2,9,2048]{3,2,0,1:T(8,128)(2,1)S(1)} fusion(bf16[2,512,2048]{2,1,0:T(8,128)(2,1)} %param.36, bf16[2,2048,512]{2,1,0:T(8,128)(2,1)} %param.35, bf16[4,2,9,2048]{3,0,2,1:T(4,128)(2,1)S(1)} %bitcast.81, f32[4,2,9,512]{3,2,0,1:T(8,128)S(1)} %fusion.14), kind=kOutput, calls=%fused_computation.8 | convolution fusion | flops 302358528 | bytes 9125888 | tf_op jit(solution)/shard_map/gecf,efd->gecd/dot_general | solution.py:110
  73.2 0.9 copy.48
  74.1 3.5 %all-to-all-start.1 = ((bf16[4,18,2048]{2,1,0:T(8,128)(2,1)}), bf16[4,18,2048]{2,1,0:T(8,128)(2,1)S(1)}, u32[]{:S(2)}, u32[]{:S(2)}) async-start(bf16[4,18,2048]{2,1,0:T(8,128)(2,1)} %copy.48), calls=%async_computation.1 | async-start | bytes 786432 | tf_op jit(solution)/shard_map/all_to_all | solution.py:121
  77.6 1.1 fusion.54
  78.7 10.1 %all-to-all-done.1 = bf16[4,18,2048]{2,1,0:T(8,128)(2,1)S(1)} async-done(((bf16[4,18,2048]{2,1,0:T(8,128)(2,1)}), bf16[4,18,2048]{2,1,0:T(8,128)(2,1)S(1)}, u32[]{:S(2)}, u32[]{:S(2)}) %all-to-all-start.1) | async-done | bytes 294944 | tf_op jit(solution)/shard_map/all_to_all | solution.py:121
  89.2 2.0 %fusion.12 = bf16[12,2048]{1,0:T(8,128)(2,1)} fusion(f32[12,2048]{1,0:T(8,128)S(1)} %fusion.53, bf16[64,2048]{1,0:T(8,128)(2,1)S(1)} %copy-done.2, bf16[12,2048]{1,0:T(8,128)(2,1)S(1)} %add_convert_fusion, bf16[2048,64]{0,1:T(8,128)(2,1)} %param.38, f32[12,64]{1,0:T(8,128)S(1)} %fusion.54), kind=kOutput, calls=%fused_computation.11 | convolution fusion | flops 6345216 | bytes 723968 | tf_op jit(solution)/shard_map/dot_general | solution.py:120
  91.2 0.8 dynamic_slice.11
  92.7 28.1 %reduce-scatter.2.cloned.1.call-done = bf16[12,256]{1,0:T(8,128)(2,1)} async-done(((bf16[12,2048]{1,0:T(8,128)(2,1)}), bf16[12,256]{1,0:T(8,128)(2,1)}) %reduce-scatter.2.cloned.1.call-update) | async-done | bytes 6160 | tf_op jit(solution)/shard_map/reduce_scatter | solution.py:127
  120.9 0.8 fusion.42
  121.7 12.1 %all-reduce = (f32[12]{0:T(128)S(1)}, f32[12]{0:T(128)S(1)}) all-reduce(f32[12]{0:T(128)S(1)} %get-tuple-element.3, f32[12]{0:T(128)S(1)} %get-tuple-element.2), channel_id=1, replica_groups=mesh['ep'=4,'tp'=8] {'tp'}, use_global_device_ids=true, to_apply=%region_12.13 | all-reduce | flops 24 | bytes 192 | tf_op jit(solution)/shard_map/psum | solution.py:131
  133.8 1.4 add_convert_fusion.1
  (53 shorter events, 4.0 us)
Async XLA Ops:
  7.2 29.6 %copy-start = (bf16[512,2048]{1,0:T(8,128)(2,1)S(1)}, bf16[512,2048]{1,0:T(8,128)(2,1)}, u32[]{:S(2)}) copy-start(bf16[512,2048]{1,0:T(8,128)(2,1)} %param.29) | copy-start | bytes 6291460
  22.1 6.1 %copy-start.3 = (f32[4,128]{1,0:T(4,128)S(1)}, f32[4,128]{1,0:T(4,128)}, u32[]{:S(2)}) copy-start(f32[4,128]{1,0:T(4,128)} %param.23) | copy-start | bytes 6148
  32.1 1.7 %copy-start.1 = (f32[12,4,128,128]{3,2,1,0:T(8,128)}, f32[12,4,128,128]{3,2,1,0:T(8,128)S(1)}, u32[]{:S(2)}) copy-start(f32[12,4,128,128]{3,2,1,0:T(8,128)S(1)} %multiply_add_fusion) | copy-start | bytes 9437188
  32.1 4.5 %copy-start.6 = (f32[128]{0:T(128)S(1)}, f32[128]{0:T(128)}, u32[]{:S(2)}) copy-start(f32[128]{0:T(128)} %param.28) | copy-start | bytes 1540
  33.7 13.6 %copy-start.4 = (f32[2048]{0:T(1024)S(1)}, f32[2048]{0:T(1024)}, u32[]{:S(2)}) copy-start(f32[2048]{0:T(1024)} %param.31) | copy-start | bytes 24580
  33.7 13.7 %copy-start.5 = (f32[2048]{0:T(1024)S(1)}, f32[2048]{0:T(1024)}, u32[]{:S(2)}) copy-start(f32[2048]{0:T(1024)} %param.30) | copy-start | bytes 24580
  72.9 16.3 %copy-start.2 = (bf16[64,2048]{1,0:T(8,128)(2,1)S(1)}, bf16[64,2048]{1,0:T(8,128)(2,1)}, u32[]{:S(2)}) copy-start(bf16[64,2048]{1,0:T(8,128)(2,1)} %param.39) | copy-start | bytes 786436
  74.1 14.8 %all-to-all-start.1 = ((bf16[4,18,2048]{2,1,0:T(8,128)(2,1)}), bf16[4,18,2048]{2,1,0:T(8,128)(2,1)S(1)}, u32[]{:S(2)}, u32[]{:S(2)}) async-start(bf16[4,18,2048]{2,1,0:T(8,128)(2,1)} %copy.48), calls=%async_computation.1 | async-start | bytes 786432 | tf_op jit(solution)/shard_map/all_to_all | solution.py:121
  77.5 43.3 %reduce-scatter.2.cloned.1.call-start = ((), (), s32[]{:S(2)}) async-start(), calls=%async_computation.3 | async-start | bytes 73728 | tf_op jit(solution)/shard_map/reduce_scatter | solution.py:127
Sparse Core Ops, SparseCore 0:
  91.3 29.4 reduce-scatter.1
